TPU v7x, 512 devices: a 8x2x16 block of a 8x16x16 slice. The times are simulated.
512 devices in a mesh: grp: 2 (over y), sp: 16 (over z), tp: 16 (over x, core).
Axes of the slice: x: 8, y: 2, z: 16, core: 2. Of those that a mesh axis runs over, the one named last changes fastest.
The devices are a block of a 8x16x16 slice.
Arguments:
- hidden_in: bfloat16 [20480, 4096], P(('grp', 'sp'), 'tp'), parts along dimension 0, may hold values from -64 to 64
- norm_gain: float32 [2, 4096], replicated, may hold values from 0.1 to 1.9
- w_pool_in: bfloat16 [2, 4096, 1024], P(None, 'sp', 'tp'), may hold values from -0.09375 to 0.09375
- w_pool_gate: bfloat16 [2, 4096, 1024], P(None, 'sp', 'tp'), may hold values from -0.09375 to 0.09375
- group_mix: bfloat16 [2, 16, 64, 64], replicated, may hold values from -0.75 to 0.75
- w_out: bfloat16 [2, 1024, 4096], P(None, 'sp', 'tp'), may hold values from -0.1875 to 0.1875
Outputs:
- hidden_out: bfloat16 [20480, 4096], P(('grp', 'sp'), 'tp'), parts along dimension 0
There are 2 independent parts, one for each index of `grp`. A program takes and returns all parts, laid end to end along the dimension named above; an argument that names none is the same for every part. Nothing has to cross between parts.
All inputs are finite; a program needn't handle non-finite values.
Results may differ from a plain program's by a relative error of at most 0.012.
Values may be sent and summed in bfloat16 or wider, within the bound.
No kernel may reach another device: no remote copies, remote signals or barrier semaphores. Data moves between devices by JAX's collectives and lax.ppermute only.
A program may use at most 64 MiB of HBM per device.

v0:
```python
import jax
import jax.numpy as jnp
from jax import lax
from jax.experimental import pallas as pl
from jax.experimental.pallas import tpu as pltpu
from jax.sharding import PartitionSpec as P

CORES = 2
REACH = 8
PAIR = 4
norm_eps = 1e-06
bf16 = jnp.bfloat16
f32 = jnp.float32


def sent_to_all(array, axis):
    copies = jnp.broadcast_to(array, (lax.axis_size(axis), *array.shape))
    return lax.all_to_all(copies, axis, split_axis=0, concat_axis=0, tiled=True)


def exchanged(copies, axis):
    return lax.all_to_all(copies, axis, split_axis=0, concat_axis=0, tiled=True)


def swap_cores(array):
    size = lax.axis_size("tp")
    return lax.ppermute(array, "tp", [(i, i ^ 1) for i in range(size)])


def shifted_over_chips(array, step):
    size = lax.axis_size("tp")
    return lax.ppermute(array, "tp", [(i, (i + CORES * step) % size) for i in range(size)])


def same_core_blocks(block):
    chips = lax.axis_size("tp") // CORES
    chip = lax.axis_index("tp") // CORES
    out = jnp.zeros((chips, *block.shape), block.dtype)
    origin = (0,) * block.ndim
    out = lax.dynamic_update_slice(out, block[None], (chip, *origin))
    right = left = block
    for step in range(1, chips // 2 + 1):
        right = shifted_over_chips(right, 1)
        out = lax.dynamic_update_slice(out, right[None], ((chip - step) % chips, *origin))
        if step < chips - chips // 2:
            left = shifted_over_chips(left, -1)
            out = lax.dynamic_update_slice(out, left[None], ((chip + step) % chips, *origin))
    return out


def dot0(left, right):
    return lax.dot_general(left, right, (((0,), (0,)), ((), ())), preferred_element_type=f32)


def window(array, start, length):
    return lax.slice_in_dim(array, start, start + length, axis=1)


def pack_kernel(at, w_gate, w_in, w_last, gain, packed):
    layers, chans, _ = w_gate.shape
    rows = 0
    for layer in range(layers):
        for weight in (w_gate, w_in):
            packed[rows : rows + chans] = (weight[layer].astype(f32) * gain[layer : layer + 1]).astype(bf16)
            rows += chans
    for layer in range(layers):
        packed[rows : rows + w_last.shape[1]] = w_last[layer]
        rows += w_last.shape[1]


def packed_weights(w_gate, w_in, w_last, gain, row_rank):
    layers, chans, depth = w_gate.shape
    rows = layers * (2 * chans + w_last.shape[1])

    def whole(array):
        return pl.BlockSpec(array.shape, lambda step, at: (0, 0, 0))

    return pl.pallas_call(
        pack_kernel,
        grid_spec=pltpu.PrefetchScalarGridSpec(
            num_scalar_prefetch=1,
            grid=(1,),
            in_specs=[
                whole(w_gate),
                whole(w_in),
                whole(w_last),
                pl.BlockSpec((layers, depth), lambda step, at: (0, at[0])),
            ],
            out_specs=pl.BlockSpec((rows, depth), lambda step, at: (0, 0)),
        ),
        out_shape=jax.ShapeDtypeStruct((rows, depth), bf16),
        name="packed_weights",
    )(row_rank.reshape(1).astype(jnp.int32), w_gate, w_in, w_last, gain)


def squares_kernel(full_width, mine, other, scaling, squares):
    step = pl.program_id(0)
    lanes = squares.shape[1]

    @pl.when(step == 0)
    def _():
        squares[...] = jnp.zeros_like(squares)

    total = squares[...]
    for block, first in ((mine, PAIR * step), (other, 0)):
        for chip in range(PAIR):
            for i in range(0, block.shape[2], lanes):
                part = block[first + chip, :, i : i + lanes].astype(f32)
                total = total + part * part
    squares[...] = total

    @pl.when(step == pl.num_programs(0) - 1)
    def _():
        mean = jnp.sum(squares[...], axis=1, keepdims=True) / full_width
        scaling[...] = jnp.broadcast_to(lax.rsqrt(mean + norm_eps), scaling.shape)


def row_scaling(mine, other, full_width):
    chips, count, depth = mine.shape
    specs = [pl.BlockSpec(memory_space=pltpu.VMEM), pl.BlockSpec((PAIR, count, depth), lambda step: (step, 0, 0))]
    return pl.pallas_call(
        lambda *refs: squares_kernel(full_width, *refs),
        grid=(chips // PAIR,),
        in_specs=specs,
        out_specs=pl.BlockSpec((count, 128), lambda step: (0, 0)),
        scratch_shapes=[pltpu.VMEM((count, 128), f32)],
        out_shape=jax.ShapeDtypeStruct((count, 128), f32),
        compiler_params=pltpu.CompilerParams(dimension_semantics=("arbitrary",), vmem_limit_bytes=28 << 20),
        cost_estimate=pl.CostEstimate(
            flops=4 * CORES * chips * count * depth, bytes_accessed=CORES * chips * count * depth * 2, transcendentals=0
        ),
        name="row_scaling",
    )(mine, other)


def first_kernel(chans, rows, ext_rows, total_rows, at, mine, other, scaling, w_all, mix, branch, ahead, joint, acc, turned):
    step = pl.program_id(0)
    lanes = 2 * chans
    count = mine.shape[1]
    core = at[0]
    total = 0
    for chip in range(PAIR):
        for part, place in ((mine[PAIR * step + chip], core), (other[chip], 1 - core)):
            weight = w_all[CORES * chip + place]
            total = total + lax.dot_general(
                part, weight, (((1,), (1,)), ((), ())), preferred_element_type=f32
            )

    @pl.when(step == 0)
    def _():
        acc[...] = total

    @pl.when(step > 0)
    def _():
        acc[...] += total

    @pl.when(step == pl.num_programs(0) - 1)
    def _():
        code = at[1]
        both = (acc[:, :lanes] * scaling[...]).astype(bf16).astype(f32)
        running = both
        total = None
        for code_value, size in enumerate((1, 2, 4, 8)):
            running = running + pltpu.roll(running, count - size, 0)
            picked = pltpu.roll(running, size, 0)
            total = picked if total is None else jnp.where(code == code_value, picked, total)
        position = at[2] + lax.broadcasted_iota(jnp.int32, (count, lanes), 0)
        half = jnp.left_shift(1, code)
        counted = jnp.minimum(position + half, total_rows) - jnp.maximum(position - half, 0)
        counted = jnp.maximum(counted, 1).astype(f32)
        pooled = (total / counted - both).astype(bf16)
        mixed = jnp.dot(pooled, mix[...], preferred_element_type=f32)
        gated = mixed * (both / (1.0 + jnp.exp(-both)))
        turned[:count] = pltpu.roll(gated, count - REACH, 0)
        branch[...] = turned[...].T[:chans, :rows].astype(bf16)
        turned[:count] = pltpu.roll(acc[:, lanes:], count - REACH, 0)
        ahead[...] = turned[...].T[:, :rows]
        own = acc[ext_rows:, lanes:].astype(bf16)
        for i in range(joint.shape[0]):
            joint[i] = own


def first_layer(mine, other, scaling, gathered, mix, at, chans, ext_rows, total_rows, sp_size):
    chips, count, depth = mine.shape
    lanes = 2 * chans
    rows = ext_rows - 2 * REACH
    padded = -(-count // 128) * 128

    def block(step, at):
        return (step, 0, 0)

    def whole(step, at):
        return (0, 0)

    return pl.pallas_call(
        lambda *refs: first_kernel(chans, rows, ext_rows, total_rows, *refs),
        grid_spec=pltpu.PrefetchScalarGridSpec(
            num_scalar_prefetch=1,
            grid=(chips // PAIR,),
            in_specs=[
                pl.BlockSpec(memory_space=pltpu.VMEM),
                pl.BlockSpec((PAIR, count, depth), block),
                pl.BlockSpec((count, lanes), whole),
                pl.BlockSpec((CORES * PAIR, 2 * lanes, depth), block),
                pl.BlockSpec((lanes, lanes), whole),
            ],
            out_specs=[
                pl.BlockSpec((chans, rows), whole),
                pl.BlockSpec((lanes, rows), whole),
                pl.BlockSpec((sp_size, count - ext_rows, lanes), lambda step, at: (0, 0, 0)),
            ],
            scratch_shapes=[
                pltpu.VMEM((count, 2 * lanes), f32),
                pltpu.VMEM((padded, lanes), f32),
            ],
        ),
        out_shape=[
            jax.ShapeDtypeStruct((chans, rows), bf16),
            jax.ShapeDtypeStruct((lanes, rows), f32),
            jax.ShapeDtypeStruct((sp_size, count - ext_rows, lanes), bf16),
        ],
        compiler_params=pltpu.CompilerParams(dimension_semantics=("arbitrary",), vmem_limit_bytes=46 << 20),
        cost_estimate=pl.CostEstimate(
            flops=CORES * chips * count * depth * 4 * lanes,
            bytes_accessed=CORES * chips * depth * 2 * (count + 2 * lanes),
            transcendentals=0,
        ),
        name="first_layer",
    )(at, mine, other, scaling, gathered, mix)


def mixed_branch(sums, scaling, mix, first_position, total_rows, code):
    rows = sums.shape[1] - 2 * REACH
    chans = sums.shape[0] // 2
    scaled = (sums * scaling[None, :]).astype(bf16).astype(f32)
    pool_in = scaled[chans:]
    gate = window(scaled[:chans], REACH, rows)
    position = first_position + jnp.arange(rows, dtype=jnp.int32)
    half = jnp.left_shift(1, code)
    counted = jnp.minimum(position + half, total_rows) - jnp.maximum(position - half, 0)
    counted = counted.astype(f32)
    running = pool_in
    total = None
    for code_value, size in enumerate((1, 2, 4, 8)):
        width = running.shape[1] - size
        running = window(running, 0, width) + window(running, size, width)
        picked = window(running, REACH - size, rows)
        total = picked if total is None else jnp.where(code == code_value, picked, total)
    pooled = (total / counted[None, :] - window(pool_in, REACH, rows)).astype(bf16)
    mixed = dot0(mix, pooled)
    return (mixed * jax.nn.silu(gate)).astype(bf16)


def local(hidden_in, norm_gain, w_pool_in, w_pool_gate, group_mix, w_out):
    rows, cols = hidden_in.shape
    chans = w_pool_in.shape[2]
    out_rows = w_out.shape[1]
    col_rank = lax.axis_index("tp")
    row_rank = lax.axis_index("sp")
    tp_size = lax.axis_size("tp")
    sp_size = lax.axis_size("sp")
    chips = tp_size // CORES
    core = jnp.bitwise_and(col_rank, CORES - 1)
    total_rows = rows * sp_size
    full_width = cols * tp_size
    code = jnp.bitwise_and(col_rank, 3)
    halo = 2 * REACH
    ext_rows = rows + 2 * halo
    lanes = 2 * chans

    packed = packed_weights(w_pool_gate.transpose(0, 2, 1), w_pool_in.transpose(0, 2, 1), w_out, norm_gain, row_rank)
    packed, hidden_in = lax.optimization_barrier((packed, hidden_in))
    gathered = lax.all_gather(packed, "sp", axis=0, tiled=False)

    def last_rows(gathered, layer):
        at = 2 * lanes + layer * out_rows
        return gathered[:, at : at + out_rows].reshape(chips, CORES * out_rows, cols)

    up = [(i, i + 1) for i in range(sp_size - 1)]
    down = [(j, i) for i, j in up]
    before = lax.ppermute(hidden_in[rows - halo :], "sp", up)
    after = lax.ppermute(hidden_in[:halo], "sp", down)
    block = jnp.concatenate([before, hidden_in, after, w_out[0]], axis=0)
    mine = same_core_blocks(block)
    other = swap_cores(mine)

    chip = col_rank // CORES
    ring = jnp.bitwise_and(chip + core, 1)

    def by_ring(array):
        size = array.shape[1] // CORES
        paired = array.reshape(chips // 2, 2 * CORES, size, array.shape[2])
        sides = []
        for c in (ring, 1 - ring):
            picked = [lax.dynamic_slice_in_dim(paired, at, 1, axis=1) for at in (c, CORES + 1 - c)]
            sides.append(jnp.concatenate(picked, axis=1).reshape(-1, array.shape[2]))
        return sides

    twins = [[CORES * i + (i + c) % CORES for i in range(chips)] for c in range(CORES)]

    def over_twins(branch):
        return lax.all_gather(branch, "tp", axis=0, tiled=True, axis_index_groups=twins)

    def product(weights, operands):
        return sum(dot0(weight, operand) for weight, operand in zip(weights, operands))

    mixes = [lax.dynamic_index_in_dim(group_mix[i], col_rank, 0, keepdims=False) for i in range(2)]

    mid_rows = rows + 2 * REACH
    start = row_rank * rows
    mix = jnp.pad(mixes[0], ((chans, 0), (0, chans)))
    scalars = jnp.stack([core, code, start - halo]).astype(jnp.int32)
    scaling = row_scaling(mine, other, full_width)
    branch, ahead, joint = first_layer(
        mine, other, scaling, gathered, mix, scalars, chans, ext_rows, total_rows, sp_size
    )
    joint = exchanged(joint, "sp")
    same = over_twins(branch)
    same, joint, gathered = lax.optimization_barrier((same, joint, gathered))
    joint = joint.reshape(chips, CORES * out_rows, lanes)
    other = swap_cores(same)
    pair = same, other
    delta = product(pair, by_ring(last_rows(gathered, 0)))
    resid = (block[REACH : REACH + mid_rows].astype(f32) + delta).astype(bf16)
    resid_f = resid.astype(f32)
    square_sum = sent_to_all(jnp.sum(resid_f * resid_f, axis=1), "tp").sum(axis=0)
    scaling = lax.rsqrt(square_sum / full_width + norm_eps)

    sums = ahead + product(by_ring(joint), pair)
    branch = mixed_branch(sums, scaling, mixes[1], start, total_rows, code)
    same = over_twins(branch)
    pair = same, swap_cores(same)
    resid = resid_f[REACH : REACH + rows] + product(pair, by_ring(last_rows(gathered, 1)))
    return resid.astype(bf16)


def solution(mesh):
    in_specs = (
        P(("grp", "sp"), "tp"),
        P(),
        P(None, "sp", "tp"),
        P(None, "sp", "tp"),
        P(),
        P(None, "sp", "tp"),
    )
    out_specs = P(("grp", "sp"), "tp")
    return jax.shard_map(local, mesh=mesh, in_specs=in_specs, out_specs=out_specs, check_vma=False)
```

profile of v0, /device:TPU:65, one launch (start us, length us, event | category | flops | bytes accessed | tf_op | source)
XLA Modules:
  0.0 219.3 jit_solution(9913059238069667471)
XLA Ops:
  6.6 1.7 packed_weights.1
  9.0 6.6 %collective-permute-start = (bf16[16,256]{1,0:T(8,128)(2,1)S(1)}, bf16[16,256]{1,0:T(8,128)(2,1)S(1)}, u32[]{:S(2)}, u32[]{:S(2)}) collective-permute-start(bf16[16,256]{1,0:T(8,128)(2,1)S(1)} %get-tuple-element.35), channel_id=1, source_target_pairs={{0,16},{16,32},{32,48},{48,64},{64,80},{80,96},{96,112},{112,128},... | collective-permute-start | bytes 24584 | tf_op jit(solution)/shard_map/ppermute | solution.py:281
  15.5 1.3 collective-permute-start.1
  17.6 4.7 %collective-permute-done.1 = bf16[16,256]{1,0:T(8,128)(2,1)S(1)} collective-permute-done((bf16[16,256]{1,0:T(8,128)(2,1)S(1)}, bf16[16,256]{1,0:T(8,128)(2,1)S(1)}, u32[]{:S(2)}, u32[]{:S(2)}) %collective-permute-start.1) | collective-permute-done | bytes 8224 | tf_op jit(solution)/shard_map/ppermute | solution.py:282
  22.3 1.7 pad_maximum_fusion
  24.1 3.3 %collective-permute-start.2 = (bf16[736,256]{1,0:T(8,128)(2,1)}, bf16[736,256]{1,0:T(8,128)(2,1)}, u32[]{:S(2)}, u32[]{:S(2)}) collective-permute-start(bf16[736,256]{1,0:T(8,128)(2,1)} %pad_maximum_fusion), channel_id=1, source_target_pairs={{0,2},{1,3},{2,4},{3,5},{4,6},{5,7},{6,8},{7,9},{8,10},{9,11},{10,... | collective-permute-start | bytes 1130504 | tf_op jit(solution)/shard_map/ppermute | solution.py:32
  27.4 4.1 %collective-permute-start.3 = (bf16[736,256]{1,0:T(8,128)(2,1)}, bf16[736,256]{1,0:T(8,128)(2,1)}, u32[]{:S(2)}, u32[]{:S(2)}) collective-permute-start(bf16[736,256]{1,0:T(8,128)(2,1)} %pad_maximum_fusion), channel_id=1, source_target_pairs={{0,14},{1,15},{2,0},{3,1},{4,2},{5,3},{6,4},{7,5},{8,6},{9,7},{10,... | collective-permute-start | bytes 1130504 | tf_op jit(solution)/shard_map/ppermute | solution.py:32
  31.9 2.9 %collective-permute-done.2 = bf16[736,256]{1,0:T(8,128)(2,1)} collective-permute-done((bf16[736,256]{1,0:T(8,128)(2,1)}, bf16[736,256]{1,0:T(8,128)(2,1)}, u32[]{:S(2)}, u32[]{:S(2)}) %collective-permute-start.2) | collective-permute-done | bytes 376864 | tf_op jit(solution)/shard_map/ppermute | solution.py:32
  34.8 2.4 %collective-permute-start.4 = (bf16[736,256]{1,0:T(8,128)(2,1)}, bf16[736,256]{1,0:T(8,128)(2,1)S(1)}, u32[]{:S(2)}, u32[]{:S(2)}) collective-permute-start(bf16[736,256]{1,0:T(8,128)(2,1)} %collective-permute-done.2), channel_id=1, source_target_pairs={{0,2},{1,3},{2,4},{3,5},{4,6},{5,7},{6,8},{7,9},{8,10},{9,11},{10,... | collective-permute-start | bytes 1130504 | tf_op jit(solution)/shard_map/ppermute | solution.py:32
  37.3 5.0 %collective-permute-start.5 = (bf16[736,256]{1,0:T(8,128)(2,1)}, bf16[736,256]{1,0:T(8,128)(2,1)S(1)}, u32[]{:S(2)}, u32[]{:S(2)}) collective-permute-start(bf16[736,256]{1,0:T(8,128)(2,1)} %collective-permute-done.3), channel_id=1, source_target_pairs={{0,14},{1,15},{2,0},{3,1},{4,2},{5,3},{6,4},{7,5},{8,6},{9,7},{10,... | collective-permute-start | bytes 1130504 | tf_op jit(solution)/shard_map/ppermute | solution.py:32
  44.4 1.2 collective-permute-done.4
  45.5 1.9 collective-permute-start.6
  47.5 4.6 %collective-permute-start.7 = (bf16[736,256]{1,0:T(8,128)(2,1)S(1)}, bf16[736,256]{1,0:T(8,128)(2,1)S(1)}, u32[]{:S(2)}, u32[]{:S(2)}) collective-permute-start(bf16[736,256]{1,0:T(8,128)(2,1)S(1)} %collective-permute-done.5), channel_id=1, source_target_pairs={{0,14},{1,15},{2,0},{3,1},{4,2},{5,3},{6,4},{7,5},{8,6},{9,7},{10,... | collective-permute-start | bytes 1130504 | tf_op jit(solution)/shard_map/ppermute | solution.py:32
  52.2 2.9 %collective-permute-done.6 = bf16[736,256]{1,0:T(8,128)(2,1)S(1)} collective-permute-done((bf16[736,256]{1,0:T(8,128)(2,1)S(1)}, bf16[736,256]{1,0:T(8,128)(2,1)S(1)}, u32[]{:S(2)}, u32[]{:S(2)}) %collective-permute-start.6) | collective-permute-done | bytes 376864 | tf_op jit(solution)/shard_map/ppermute | solution.py:32
  55.1 1.9 collective-permute-start.8
  57.1 7.5 %collective-permute-done.8 = bf16[736,256]{1,0:T(8,128)(2,1)S(1)} collective-permute-done((bf16[736,256]{1,0:T(8,128)(2,1)S(1)}, bf16[736,256]{1,0:T(8,128)(2,1)S(1)}, u32[]{:S(2)}, u32[]{:S(2)}) %collective-permute-start.8) | collective-permute-done | bytes 376864 | tf_op jit(solution)/shard_map/ppermute | solution.py:32
  64.7 39.7 %collective-permute-start.9 = (bf16[8,736,256]{2,1,0:T(8,128)(2,1)S(1)}, bf16[8,736,256]{2,1,0:T(8,128)(2,1)}, u32[]{:S(2)}, u32[]{:S(2)}) collective-permute-start(bf16[8,736,256]{2,1,0:T(8,128)(2,1)S(1)} %bitcast_dynamic-update-slice_fusion.refs_0_.refs_1_), channel_id=1, source_target_pairs={{0,1},{1,0},{2,3},{3,2},{4,5},{5,4},{6,7},{7,6},{8,9},{9,8},{10,11... | collective-permute-start | bytes 9043976 | tf_op jit(solution)/shard_map/ppermute | solution.py:27
  105.3 4.4 %collective-permute-done.9.refs_1_.refs_2_ = bf16[8,736,256]{2,1,0:T(8,128)(2,1)} collective-permute-done((bf16[8,736,256]{2,1,0:T(8,128)(2,1)S(1)}, bf16[8,736,256]{2,1,0:T(8,128)(2,1)}, u32[]{:S(2)}, u32[]{:S(2)}) %collective-permute-start.9) | collective-permute-done | bytes 3014688 | tf_op jit(solution)/shard_map/ppermute | solution.py:27
  109.6 2.8 %row_scaling.1.refs_3_ = f32[736,128]{1,0:T(8,128)S(1)} custom-call(bf16[8,736,256]{2,1,0:T(8,128)(2,1)S(1)} %bitcast_dynamic-update-slice_fusion.refs_0_.refs_1_, bf16[8,736,256]{2,1,0:T(8,128)(2,1)} %collective-permute-done.9.refs_1_.refs_2_), custom_call_target="tpu_custom_call" | custom-call | flops 12058624 | bytes 6029312 | tf_op jit(solution)/shard_map/row_scaling/pallas_call | solution.py:121
  112.8 5.1 %first_layer.1 = (bf16[64,656]{1,0:T(8,128)(2,1)S(1)}, f32[128,656]{1,0:T(8,128)S(1)}, bf16[16,64,128]{2,1,0:T(8,128)(2,1)S(1)}) custom-call(s32[3]{0:T(128)S(1)} %pad_add_fusion.refs_0_, bf16[8,736,256]{2,1,0:T(8,128)(2,1)S(1)} %bitcast_dynamic-update-slice_fusion.refs_0_.refs_1_, bf16[8,736,256]{2,1,0:T(8,128)(2,1)} %collective-permute-done.9.refs_1_.refs_2_, ...), custom_call_target="tpu_custom_call" | custom-call | flops 1543503872 | bytes 8126464 | tf_op jit(solution)/shard_map/first_layer/pallas_call | solution.py:195
  119.3 8.9 %all-to-all-start = ((bf16[16,64,128]{2,1,0:T(8,128)(2,1)}), bf16[16,64,128]{2,1,0:T(8,128)(2,1)S(1)}, u32[]{:S(2)}, u32[]{:S(2)}) async-start(bf16[16,64,128]{2,1,0:T(8,128)(2,1)} %copy-done.2), calls=%async_computation | async-start | bytes 524288 | tf_op jit(solution)/shard_map/all_to_all | solution.py:22
  128.3 31.9 %all_gather.14 = bf16[512,656]{1,0:T(8,128)(2,1)S(1)} all-gather(bf16[64,656]{1,0:T(8,128)(2,1)S(1)} %get-tuple-element.15), channel_id=1, replica_groups={{0,3,4,7,8,11,12,15},{1,2,5,6,9,10,13,14},{16,19,20,23,24,27,28,31},{17..., dimensions={0}, use_global_device_ids=true | all-gather | bytes 755712 | tf_op jit(solution)/shard_map/all_gather | solution.py:302
  160.2 1.3 fusion.16
  161.6 1.1 copy.15
  162.7 2.5 %collective-permute-start.10 = (bf16[512,656]{0,1:T(8,128)(2,1)}, bf16[512,656]{0,1:T(8,128)(2,1)S(1)}, u32[]{:S(2)}, u32[]{:S(2)}) collective-permute-start(bf16[512,656]{0,1:T(8,128)(2,1)} %copy.15), channel_id=1, source_target_pairs={{0,1},{1,0},{2,3},{3,2},{4,5},{5,4},{6,7},{7,6},{8,9},{9,8},{10,11... | collective-permute-start | bytes 2015240 | tf_op jit(solution)/shard_map/ppermute | solution.py:27
  168.2 6.0 %all-to-all-start.1 = ((f32[16,1,656]{2,1,0:T(1,128)}), f32[16,1,656]{2,1,0:T(1,128)S(1)}, u32[]{:S(2)}, u32[]{:S(2)}) async-start(f32[16,1,656]{2,1,0:T(1,128)} %broadcast_in_dim.41), calls=%async_computation.1 | async-start | bytes 98304 | tf_op jit(solution)/shard_map/all_to_all | solution.py:18
  174.6 7.1 %all-to-all-done.1 = f32[16,1,656]{2,1,0:T(1,128)S(1)} async-done(((f32[16,1,656]{2,1,0:T(1,128)}), f32[16,1,656]{2,1,0:T(1,128)S(1)}, u32[]{:S(2)}, u32[]{:S(2)}) %all-to-all-start.1) | async-done | bytes 42016 | tf_op jit(solution)/shard_map/all_to_all | solution.py:18
  182.3 1.1 fusion
  183.4 23.9 %all_gather.15 = bf16[512,640]{1,0:T(8,128)(2,1)S(1)} all-gather(bf16[64,640]{1,0:T(8,128)(2,1)S(1)} %fusion), channel_id=1, replica_groups={{0,3,4,7,8,11,12,15},{1,2,5,6,9,10,13,14},{16,19,20,23,24,27,28,31},{17..., dimensions={0}, use_global_device_ids=true | all-gather | bytes 737280 | tf_op jit(solution)/shard_map/all_gather | solution.py:302
  207.3 2.3 %collective-permute-start.11 = (bf16[512,640]{1,0:T(8,128)(2,1)S(1)}, bf16[512,640]{1,0:T(8,128)(2,1)S(1)}, u32[]{:S(2)}, u32[]{:S(2)}) collective-permute-start(bf16[512,640]{1,0:T(8,128)(2,1)S(1)} %all_gather.15), channel_id=1, source_target_pairs={{0,1},{1,0},{2,3},{3,2},{4,5},{5,4},{6,7},{7,6},{8,9},{9,8},{10,11... | collective-permute-start | bytes 1966088 | tf_op jit(solution)/shard_map/ppermute | solution.py:27
  210.1 1.3 collective-permute-done.11
  211.3 1.1 fusion.1
  (58 shorter events, 10.9 us)
Async XLA Ops:
  6.5 25.3 %copy-start.3 = (bf16[640,256]{1,0:T(8,128)(2,1)S(1)}, bf16[640,256]{1,0:T(8,128)(2,1)}, u32[]{:S(2)}) copy-start(bf16[640,256]{1,0:T(8,128)(2,1)} %param.6) | copy-start | bytes 983044
  6.5 106.3 %all-gather.3.cloned.1.call-start = ((), (), s32[]{:S(2)}) async-start(), calls=%async_computation.2 | async-start | bytes 3342336 | tf_op jit(solution)/shard_map/all_gather | solution.py:273
  9.0 8.6 %collective-permute-start = (bf16[16,256]{1,0:T(8,128)(2,1)S(1)}, bf16[16,256]{1,0:T(8,128)(2,1)S(1)}, u32[]{:S(2)}, u32[]{:S(2)}) collective-permute-start(bf16[16,256]{1,0:T(8,128)(2,1)S(1)} %get-tuple-element.35), channel_id=1, source_target_pairs={{0,16},{16,32},{32,48},{48,64},{64,80},{80,96},{96,112},{112,128},... | collective-permute-start | bytes 24584 | tf_op jit(solution)/shard_map/ppermute | solution.py:281
  15.5 6.8 %collective-permute-start.1 = (bf16[16,256]{1,0:T(8,128)(2,1)S(1)}, bf16[16,256]{1,0:T(8,128)(2,1)S(1)}, u32[]{:S(2)}, u32[]{:S(2)}) collective-permute-start(bf16[16,256]{1,0:T(8,128)(2,1)S(1)} %get-tuple-element.36), channel_id=1, source_target_pairs={{16,0},{32,16},{48,32},{64,48},{80,64},{96,80},{112,96},{128,112},... | collective-permute-start | bytes 24584 | tf_op jit(solution)/shard_map/ppermute | solution.py:282
  24.1 10.8 %collective-permute-start.2 = (bf16[736,256]{1,0:T(8,128)(2,1)}, bf16[736,256]{1,0:T(8,128)(2,1)}, u32[]{:S(2)}, u32[]{:S(2)}) collective-permute-start(bf16[736,256]{1,0:T(8,128)(2,1)} %pad_maximum_fusion), channel_id=1, source_target_pairs={{0,2},{1,3},{2,4},{3,5},{4,6},{5,7},{6,8},{7,9},{8,10},{9,11},{10,... | collective-permute-start | bytes 1130504 | tf_op jit(solution)/shard_map/ppermute | solution.py:32
  27.4 9.9 %collective-permute-start.3 = (bf16[736,256]{1,0:T(8,128)(2,1)}, bf16[736,256]{1,0:T(8,128)(2,1)}, u32[]{:S(2)}, u32[]{:S(2)}) collective-permute-start(bf16[736,256]{1,0:T(8,128)(2,1)} %pad_maximum_fusion), channel_id=1, source_target_pairs={{0,14},{1,15},{2,0},{3,1},{4,2},{5,3},{6,4},{7,5},{8,6},{9,7},{10,... | collective-permute-start | bytes 1130504 | tf_op jit(solution)/shard_map/ppermute | solution.py:32
  31.9 72.5 %copy-start.5 = (bf16[2,16,64,64]{3,2,1,0:T(8,128)(2,1)S(1)}, bf16[2,16,64,64]{3,2,1,0:T(8,128)(2,1)}, u32[]{:S(2)}) copy-start(bf16[2,16,64,64]{3,2,1,0:T(8,128)(2,1)} %param.10) | copy-start | bytes 786436
  34.8 10.7 %collective-permute-start.4 = (bf16[736,256]{1,0:T(8,128)(2,1)}, bf16[736,256]{1,0:T(8,128)(2,1)S(1)}, u32[]{:S(2)}, u32[]{:S(2)}) collective-permute-start(bf16[736,256]{1,0:T(8,128)(2,1)} %collective-permute-done.2), channel_id=1, source_target_pairs={{0,2},{1,3},{2,4},{3,5},{4,6},{5,7},{6,8},{7,9},{8,10},{9,11},{10,... | collective-permute-start | bytes 1130504 | tf_op jit(solution)/shard_map/ppermute | solution.py:32
  37.3 10.2 %collective-permute-start.5 = (bf16[736,256]{1,0:T(8,128)(2,1)}, bf16[736,256]{1,0:T(8,128)(2,1)S(1)}, u32[]{:S(2)}, u32[]{:S(2)}) collective-permute-start(bf16[736,256]{1,0:T(8,128)(2,1)} %collective-permute-done.3), channel_id=1, source_target_pairs={{0,14},{1,15},{2,0},{3,1},{4,2},{5,3},{6,4},{7,5},{8,6},{9,7},{10,... | collective-permute-start | bytes 1130504 | tf_op jit(solution)/shard_map/ppermute | solution.py:32
  45.5 9.6 %collective-permute-start.6 = (bf16[736,256]{1,0:T(8,128)(2,1)S(1)}, bf16[736,256]{1,0:T(8,128)(2,1)S(1)}, u32[]{:S(2)}, u32[]{:S(2)}) collective-permute-start(bf16[736,256]{1,0:T(8,128)(2,1)S(1)} %collective-permute-done.4), channel_id=1, source_target_pairs={{0,2},{1,3},{2,4},{3,5},{4,6},{5,7},{6,8},{7,9},{8,10},{9,11},{10,... | collective-permute-start | bytes 1130504 | tf_op jit(solution)/shard_map/ppermute | solution.py:32
  47.5 9.6 %collective-permute-start.7 = (bf16[736,256]{1,0:T(8,128)(2,1)S(1)}, bf16[736,256]{1,0:T(8,128)(2,1)S(1)}, u32[]{:S(2)}, u32[]{:S(2)}) collective-permute-start(bf16[736,256]{1,0:T(8,128)(2,1)S(1)} %collective-permute-done.5), channel_id=1, source_target_pairs={{0,14},{1,15},{2,0},{3,1},{4,2},{5,3},{6,4},{7,5},{8,6},{9,7},{10,... | collective-permute-start | bytes 1130504 | tf_op jit(solution)/shard_map/ppermute | solution.py:32
  55.1 9.6 %collective-permute-start.8 = (bf16[736,256]{1,0:T(8,128)(2,1)S(1)}, bf16[736,256]{1,0:T(8,128)(2,1)S(1)}, u32[]{:S(2)}, u32[]{:S(2)}) collective-permute-start(bf16[736,256]{1,0:T(8,128)(2,1)S(1)} %collective-permute-done.6), channel_id=1, source_target_pairs={{0,2},{1,3},{2,4},{3,5},{4,6},{5,7},{6,8},{7,9},{8,10},{9,11},{10,... | collective-permute-start | bytes 1130504 | tf_op jit(solution)/shard_map/ppermute | solution.py:32
  64.7 44.9 %collective-permute-start.9 = (bf16[8,736,256]{2,1,0:T(8,128)(2,1)S(1)}, bf16[8,736,256]{2,1,0:T(8,128)(2,1)}, u32[]{:S(2)}, u32[]{:S(2)}) collective-permute-start(bf16[8,736,256]{2,1,0:T(8,128)(2,1)S(1)} %bitcast_dynamic-update-slice_fusion.refs_0_.refs_1_), channel_id=1, source_target_pairs={{0,1},{1,0},{2,3},{3,2},{4,5},{5,4},{6,7},{7,6},{8,9},{9,8},{10,11... | collective-permute-start | bytes 9043976 | tf_op jit(solution)/shard_map/ppermute | solution.py:27
  117.9 0.7 copy-start
  118.6 0.7 copy-start.2
  119.3 40.9 %all-to-all-start = ((bf16[16,64,128]{2,1,0:T(8,128)(2,1)}), bf16[16,64,128]{2,1,0:T(8,128)(2,1)S(1)}, u32[]{:S(2)}, u32[]{:S(2)}) async-start(bf16[16,64,128]{2,1,0:T(8,128)(2,1)} %copy-done.2), calls=%async_computation | async-start | bytes 524288 | tf_op jit(solution)/shard_map/all_to_all | solution.py:22
  162.7 4.5 %collective-permute-start.10 = (bf16[512,656]{0,1:T(8,128)(2,1)}, bf16[512,656]{0,1:T(8,128)(2,1)S(1)}, u32[]{:S(2)}, u32[]{:S(2)}) collective-permute-start(bf16[512,656]{0,1:T(8,128)(2,1)} %copy.15), channel_id=1, source_target_pairs={{0,1},{1,0},{2,3},{3,2},{4,5},{5,4},{6,7},{7,6},{8,9},{9,8},{10,11... | collective-permute-start | bytes 2015240 | tf_op jit(solution)/shard_map/ppermute | solution.py:27
  165.2 1.9 copy-start.4
  165.8 16.0 %copy-start.1 = (f32[128,656]{1,0:T(8,128)S(1)}, f32[128,656]{1,0:T(8,128)}, u32[]{:S(2)}) copy-start(f32[128,656]{1,0:T(8,128)} %copy-done) | copy-start | bytes 1007620
  168.2 13.5 %all-to-all-start.1 = ((f32[16,1,656]{2,1,0:T(1,128)}), f32[16,1,656]{2,1,0:T(1,128)S(1)}, u32[]{:S(2)}, u32[]{:S(2)}) async-start(f32[16,1,656]{2,1,0:T(1,128)} %broadcast_in_dim.41), calls=%async_computation.1 | async-start | bytes 98304 | tf_op jit(solution)/shard_map/all_to_all | solution.py:18
  207.3 4.0 %collective-permute-start.11 = (bf16[512,640]{1,0:T(8,128)(2,1)S(1)}, bf16[512,640]{1,0:T(8,128)(2,1)S(1)}, u32[]{:S(2)}, u32[]{:S(2)}) collective-permute-start(bf16[512,640]{1,0:T(8,128)(2,1)S(1)} %all_gather.15), channel_id=1, source_target_pairs={{0,1},{1,0},{2,3},{3,2},{4,5},{5,4},{6,7},{7,6},{8,9},{9,8},{10,11... | collective-permute-start | bytes 1966088 | tf_op jit(solution)/shard_map/ppermute | solution.py:27
Sparse Core Ops, SparseCore 0:
  9.4 103.3 all-gather.2
where the time goes:
time: 220 us; the launch traced here: 219 us
  starting transfers between devices  90.7 us (41%)
  blocking collectives  55.8 us (25%)
  waiting for transfers between devices  33.4 us (15%)
  between operations  14 us (6%)
  Pallas kernels  9.55 us (4%)
  local copies, waits for them, and re-layouts  9.38 us (4%)
  matrix products  4.05 us (2%)
  other arithmetic  2.45 us (1%)
    all_gather x2, blocking collectives, over_twins(): lax.all_gather(branch, 'tp', axis=0, tiled=True, axis_index_groups=twins)  55.8 us
    ppermute x3, starting transfers between devices, swap_cores(): return lax.ppermute(array, 'tp', [(i, i ^ 1) for i in range(size)])  44.6 us
    ppermute x7, starting transfers between devices, shifted_over_chips(): lax.ppermute(array, 'tp', [(i, (i + CORES * step) % size) for i in range(...  23.3 us
    ppermute x7, waiting for transfers between devices, shifted_over_chips(): lax.ppermute(array, 'tp', [(i, (i + CORES * step) % size) for i in range(...  14.5 us
    all_to_all x1, starting transfers between devices, exchanged(): return lax.all_to_all(copies, axis, split_axis=0, concat_axis=0, tiled=True)  8.94 us
    all_to_all x1, waiting for transfers between devices, sent_to_all(): return lax.all_to_all(copies, axis, split_axis=0, concat_axis=0, tiled=True)  7.13 us
    ppermute x3, waiting for transfers between devices, swap_cores(): return lax.ppermute(array, 'tp', [(i, i ^ 1) for i in range(size)])  6.58 us
    ppermute x1, starting transfers between devices, local(): before = lax.ppermute(hidden_in[rows - halo:], 'sp', up)  6.55 us
  transfers between devices with their start and end apart: 15, of which 10 were waited for; matrix products, arithmetic and copies ran while one was open for 4% of the time, Pallas kernels for 1%

commit v1 on v0

--- a/solution.py
+++ b/solution.py
@@ -140,7 +140,7 @@
     core = at[0]
     total = 0
     for chip in range(PAIR):
-        for part, place in ((mine[PAIR * step + chip], core), (other[chip], 1 - core)):
+        for part, place in ((mine[chip], core), (other[chip], 1 - core)):
             weight = w_all[CORES * chip + place]
             total = total + lax.dot_general(
                 part, weight, (((1,), (1,)), ((), ())), preferred_element_type=f32
@@ -198,7 +198,7 @@
             num_scalar_prefetch=1,
             grid=(chips // PAIR,),
             in_specs=[
-                pl.BlockSpec(memory_space=pltpu.VMEM),
+                pl.BlockSpec((PAIR, count, depth), block),
                 pl.BlockSpec((PAIR, count, depth), block),
                 pl.BlockSpec((count, lanes), whole),
                 pl.BlockSpec((CORES * PAIR, 2 * lanes, depth), block),
@@ -219,7 +219,7 @@
             jax.ShapeDtypeStruct((lanes, rows), f32),
             jax.ShapeDtypeStruct((sp_size, count - ext_rows, lanes), bf16),
         ],
-        compiler_params=pltpu.CompilerParams(dimension_semantics=("arbitrary",), vmem_limit_bytes=46 << 20),
+        compiler_params=pltpu.CompilerParams(dimension_semantics=("arbitrary",), vmem_limit_bytes=50 << 20),
         cost_estimate=pl.CostEstimate(
             flops=CORES * chips * count * depth * 4 * lanes,
             bytes_accessed=CORES * chips * depth * 2 * (count + 2 * lanes),

time: 220 us -> 220 us (level)
  no operation moved by 1% of the time
where the time goes in v1:
time: 220 us; the launch traced here: 219 us
  starting transfers between devices  90.7 us (41%)
  blocking collectives  55.8 us (25%)
  waiting for transfers between devices  33.4 us (15%)
  between operations  14 us (6%)
  Pallas kernels  10.8 us (5%)
  local copies, waits for them, and re-layouts  7.97 us (4%)
  matrix products  4.06 us (2%)
  other arithmetic  2.43 us (1%)
    all_gather x2, blocking collectives, over_twins(): lax.all_gather(branch, 'tp', axis=0, tiled=True, axis_index_groups=twins)  55.8 us
    ppermute x3, starting transfers between devices, swap_cores(): return lax.ppermute(array, 'tp', [(i, i ^ 1) for i in range(size)])  44.6 us
    ppermute x7, starting transfers between devices, shifted_over_chips(): lax.ppermute(array, 'tp', [(i, (i + CORES * step) % size) for i in range(...  23.3 us
    ppermute x7, waiting for transfers between devices, shifted_over_chips(): lax.ppermute(array, 'tp', [(i, (i + CORES * step) % size) for i in range(...  14.5 us
    all_to_all x1, starting transfers between devices, exchanged(): return lax.all_to_all(copies, axis, split_axis=0, concat_axis=0, tiled=True)  8.94 us
    all_to_all x1, waiting for transfers between devices, sent_to_all(): return lax.all_to_all(copies, axis, split_axis=0, concat_axis=0, tiled=True)  7.12 us
    ppermute x3, waiting for transfers between devices, swap_cores(): return lax.ppermute(array, 'tp', [(i, i ^ 1) for i in range(size)])  6.58 us
    ppermute x1, starting transfers between devices, local(): before = lax.ppermute(hidden_in[rows - halo:], 'sp', up)  6.55 us
  transfers between devices with their start and end apart: 15, of which 10 were waited for; matrix products, arithmetic and copies ran while one was open for 4% of the time, Pallas kernels for 1%

profile of v1, /device:TPU:65, one launch (start us, length us, event | category | flops | bytes accessed | tf_op | source)
XLA Modules:
  0.0 219.1 jit_solution(11551016574844558786)
XLA Ops:
  6.6 1.6 packed_weights.1
  9.0 6.6 %collective-permute-start = (bf16[16,256]{1,0:T(8,128)(2,1)S(1)}, bf16[16,256]{1,0:T(8,128)(2,1)S(1)}, u32[]{:S(2)}, u32[]{:S(2)}) collective-permute-start(bf16[16,256]{1,0:T(8,128)(2,1)S(1)} %get-tuple-element.35), channel_id=1, source_target_pairs={{0,16},{16,32},{32,48},{48,64},{64,80},{80,96},{96,112},{112,128},... | collective-permute-start | bytes 24584 | tf_op jit(solution)/shard_map/ppermute | solution.py:281
  15.5 1.3 collective-permute-start.1
  17.6 4.7 %collective-permute-done.1 = bf16[16,256]{1,0:T(8,128)(2,1)S(1)} collective-permute-done((bf16[16,256]{1,0:T(8,128)(2,1)S(1)}, bf16[16,256]{1,0:T(8,128)(2,1)S(1)}, u32[]{:S(2)}, u32[]{:S(2)}) %collective-permute-start.1) | collective-permute-done | bytes 8224 | tf_op jit(solution)/shard_map/ppermute | solution.py:282
  22.3 1.7 pad_maximum_fusion
  24.1 3.3 %collective-permute-start.2 = (bf16[736,256]{1,0:T(8,128)(2,1)}, bf16[736,256]{1,0:T(8,128)(2,1)}, u32[]{:S(2)}, u32[]{:S(2)}) collective-permute-start(bf16[736,256]{1,0:T(8,128)(2,1)} %pad_maximum_fusion), channel_id=1, source_target_pairs={{0,2},{1,3},{2,4},{3,5},{4,6},{5,7},{6,8},{7,9},{8,10},{9,11},{10,... | collective-permute-start | bytes 1130504 | tf_op jit(solution)/shard_map/ppermute | solution.py:32
  27.3 4.1 %collective-permute-start.3 = (bf16[736,256]{1,0:T(8,128)(2,1)}, bf16[736,256]{1,0:T(8,128)(2,1)}, u32[]{:S(2)}, u32[]{:S(2)}) collective-permute-start(bf16[736,256]{1,0:T(8,128)(2,1)} %pad_maximum_fusion), channel_id=1, source_target_pairs={{0,14},{1,15},{2,0},{3,1},{4,2},{5,3},{6,4},{7,5},{8,6},{9,7},{10,... | collective-permute-start | bytes 1130504 | tf_op jit(solution)/shard_map/ppermute | solution.py:32
  31.9 2.9 %collective-permute-done.2 = bf16[736,256]{1,0:T(8,128)(2,1)} collective-permute-done((bf16[736,256]{1,0:T(8,128)(2,1)}, bf16[736,256]{1,0:T(8,128)(2,1)}, u32[]{:S(2)}, u32[]{:S(2)}) %collective-permute-start.2) | collective-permute-done | bytes 376864 | tf_op jit(solution)/shard_map/ppermute | solution.py:32
  34.8 2.4 %collective-permute-start.4 = (bf16[736,256]{1,0:T(8,128)(2,1)}, bf16[736,256]{1,0:T(8,128)(2,1)S(1)}, u32[]{:S(2)}, u32[]{:S(2)}) collective-permute-start(bf16[736,256]{1,0:T(8,128)(2,1)} %collective-permute-done.2), channel_id=1, source_target_pairs={{0,2},{1,3},{2,4},{3,5},{4,6},{5,7},{6,8},{7,9},{8,10},{9,11},{10,... | collective-permute-start | bytes 1130504 | tf_op jit(solution)/shard_map/ppermute | solution.py:32
  37.3 5.0 %collective-permute-start.5 = (bf16[736,256]{1,0:T(8,128)(2,1)}, bf16[736,256]{1,0:T(8,128)(2,1)S(1)}, u32[]{:S(2)}, u32[]{:S(2)}) collective-permute-start(bf16[736,256]{1,0:T(8,128)(2,1)} %collective-permute-done.3), channel_id=1, source_target_pairs={{0,14},{1,15},{2,0},{3,1},{4,2},{5,3},{6,4},{7,5},{8,6},{9,7},{10,... | collective-permute-start | bytes 1130504 | tf_op jit(solution)/shard_map/ppermute | solution.py:32
  44.3 1.2 collective-permute-done.4
  45.5 1.9 collective-permute-start.6
  47.5 4.6 %collective-permute-start.7 = (bf16[736,256]{1,0:T(8,128)(2,1)S(1)}, bf16[736,256]{1,0:T(8,128)(2,1)S(1)}, u32[]{:S(2)}, u32[]{:S(2)}) collective-permute-start(bf16[736,256]{1,0:T(8,128)(2,1)S(1)} %collective-permute-done.5), channel_id=1, source_target_pairs={{0,14},{1,15},{2,0},{3,1},{4,2},{5,3},{6,4},{7,5},{8,6},{9,7},{10,... | collective-permute-start | bytes 1130504 | tf_op jit(solution)/shard_map/ppermute | solution.py:32
  52.2 2.9 %collective-permute-done.6 = bf16[736,256]{1,0:T(8,128)(2,1)S(1)} collective-permute-done((bf16[736,256]{1,0:T(8,128)(2,1)S(1)}, bf16[736,256]{1,0:T(8,128)(2,1)S(1)}, u32[]{:S(2)}, u32[]{:S(2)}) %collective-permute-start.6) | collective-permute-done | bytes 376864 | tf_op jit(solution)/shard_map/ppermute | solution.py:32
  55.1 1.9 collective-permute-start.8
  57.1 7.5 %collective-permute-done.8 = bf16[736,256]{1,0:T(8,128)(2,1)S(1)} collective-permute-done((bf16[736,256]{1,0:T(8,128)(2,1)S(1)}, bf16[736,256]{1,0:T(8,128)(2,1)S(1)}, u32[]{:S(2)}, u32[]{:S(2)}) %collective-permute-start.8) | collective-permute-done | bytes 376864 | tf_op jit(solution)/shard_map/ppermute | solution.py:32
  64.7 39.7 %collective-permute-start.9 = (bf16[8,736,256]{2,1,0:T(8,128)(2,1)S(1)}, bf16[8,736,256]{2,1,0:T(8,128)(2,1)}, u32[]{:S(2)}, u32[]{:S(2)}) collective-permute-start(bf16[8,736,256]{2,1,0:T(8,128)(2,1)S(1)} %bitcast_dynamic-update-slice_fusion.refs_0_.refs_1_), channel_id=1, source_target_pairs={{0,1},{1,0},{2,3},{3,2},{4,5},{5,4},{6,7},{7,6},{8,9},{9,8},{10,11... | collective-permute-start | bytes 9043976 | tf_op jit(solution)/shard_map/ppermute | solution.py:27
  105.3 4.4 %collective-permute-done.9.refs_1_.refs_2_ = bf16[8,736,256]{2,1,0:T(8,128)(2,1)} collective-permute-done((bf16[8,736,256]{2,1,0:T(8,128)(2,1)S(1)}, bf16[8,736,256]{2,1,0:T(8,128)(2,1)}, u32[]{:S(2)}, u32[]{:S(2)}) %collective-permute-start.9) | collective-permute-done | bytes 3014688 | tf_op jit(solution)/shard_map/ppermute | solution.py:27
  109.6 2.8 %row_scaling.1.refs_3_ = f32[736,128]{1,0:T(8,128)S(1)} custom-call(bf16[8,736,256]{2,1,0:T(8,128)(2,1)S(1)} %bitcast_dynamic-update-slice_fusion.refs_0_.refs_1_, bf16[8,736,256]{2,1,0:T(8,128)(2,1)} %collective-permute-done.9.refs_1_.refs_2_), custom_call_target="tpu_custom_call" | custom-call | flops 12058624 | bytes 6029312 | tf_op jit(solution)/shard_map/row_scaling/pallas_call | solution.py:121
  112.8 6.4 %first_layer.1 = (bf16[64,656]{1,0:T(8,128)(2,1)S(1)}, f32[128,656]{1,0:T(8,128)S(1)}, bf16[16,64,128]{2,1,0:T(8,128)(2,1)}) custom-call(s32[3]{0:T(128)S(1)} %pad_add_fusion.refs_0_, bf16[8,736,256]{2,1,0:T(8,128)(2,1)} %copy-done, bf16[8,736,256]{2,1,0:T(8,128)(2,1)} %collective-permute-done.9.refs_1_.refs_2_, f32[736,128]{1,0:T(8,128)S(1)} %row_scaling.1.refs_3_, ...), custom_call_target="tpu_custom_call" | custom-call | flops 1543503872 | bytes 8126464 | tf_op jit(solution)/shard_map/first_layer/pallas_call | solution.py:195
  119.2 8.9 %all-to-all-start = ((bf16[16,64,128]{2,1,0:T(8,128)(2,1)}), bf16[16,64,128]{2,1,0:T(8,128)(2,1)S(1)}, u32[]{:S(2)}, u32[]{:S(2)}) async-start(bf16[16,64,128]{2,1,0:T(8,128)(2,1)} %get-tuple-element.16), calls=%async_computation | async-start | bytes 524288 | tf_op jit(solution)/shard_map/all_to_all | solution.py:22
  128.2 31.9 %all_gather.14 = bf16[512,656]{1,0:T(8,128)(2,1)S(1)} all-gather(bf16[64,656]{1,0:T(8,128)(2,1)S(1)} %get-tuple-element.15), channel_id=1, replica_groups={{0,3,4,7,8,11,12,15},{1,2,5,6,9,10,13,14},{16,19,20,23,24,27,28,31},{17..., dimensions={0}, use_global_device_ids=true | all-gather | bytes 755712 | tf_op jit(solution)/shard_map/all_gather | solution.py:302
  160.1 1.3 fusion.16
  161.4 1.1 copy.15
  162.5 2.5 %collective-permute-start.10 = (bf16[512,656]{0,1:T(8,128)(2,1)}, bf16[512,656]{0,1:T(8,128)(2,1)S(1)}, u32[]{:S(2)}, u32[]{:S(2)}) collective-permute-start(bf16[512,656]{0,1:T(8,128)(2,1)} %copy.15), channel_id=1, source_target_pairs={{0,1},{1,0},{2,3},{3,2},{4,5},{5,4},{6,7},{7,6},{8,9},{9,8},{10,11... | collective-permute-start | bytes 2015240 | tf_op jit(solution)/shard_map/ppermute | solution.py:27
  168.1 6.0 %all-to-all-start.1 = ((f32[16,1,656]{2,1,0:T(1,128)}), f32[16,1,656]{2,1,0:T(1,128)S(1)}, u32[]{:S(2)}, u32[]{:S(2)}) async-start(f32[16,1,656]{2,1,0:T(1,128)} %broadcast_in_dim.41), calls=%async_computation.1 | async-start | bytes 98304 | tf_op jit(solution)/shard_map/all_to_all | solution.py:18
  174.4 7.1 %all-to-all-done.1 = f32[16,1,656]{2,1,0:T(1,128)S(1)} async-done(((f32[16,1,656]{2,1,0:T(1,128)}), f32[16,1,656]{2,1,0:T(1,128)S(1)}, u32[]{:S(2)}, u32[]{:S(2)}) %all-to-all-start.1) | async-done | bytes 42016 | tf_op jit(solution)/shard_map/all_to_all | solution.py:18
  182.1 1.1 fusion
  183.2 23.9 %all_gather.15 = bf16[512,640]{1,0:T(8,128)(2,1)S(1)} all-gather(bf16[64,640]{1,0:T(8,128)(2,1)S(1)} %fusion), channel_id=1, replica_groups={{0,3,4,7,8,11,12,15},{1,2,5,6,9,10,13,14},{16,19,20,23,24,27,28,31},{17..., dimensions={0}, use_global_device_ids=true | all-gather | bytes 737280 | tf_op jit(solution)/shard_map/all_gather | solution.py:302
  207.1 2.3 %collective-permute-start.11 = (bf16[512,640]{1,0:T(8,128)(2,1)S(1)}, bf16[512,640]{1,0:T(8,128)(2,1)S(1)}, u32[]{:S(2)}, u32[]{:S(2)}) collective-permute-start(bf16[512,640]{1,0:T(8,128)(2,1)S(1)} %all_gather.15), channel_id=1, source_target_pairs={{0,1},{1,0},{2,3},{3,2},{4,5},{5,4},{6,7},{7,6},{8,9},{9,8},{10,11... | collective-permute-start | bytes 1966088 | tf_op jit(solution)/shard_map/ppermute | solution.py:27
  209.9 1.3 collective-permute-done.11
  211.2 1.1 fusion.1
  (54 shorter events, 9.5 us)
Async XLA Ops:
  6.5 25.3 %copy-start.1 = (bf16[640,256]{1,0:T(8,128)(2,1)S(1)}, bf16[640,256]{1,0:T(8,128)(2,1)}, u32[]{:S(2)}) copy-start(bf16[640,256]{1,0:T(8,128)(2,1)} %param.6) | copy-start | bytes 983044
  6.5 106.3 %all-gather.3.cloned.1.call-start = ((), (), s32[]{:S(2)}) async-start(), calls=%async_computation.2 | async-start | bytes 3342336 | tf_op jit(solution)/shard_map/all_gather | solution.py:273
  9.0 8.6 %collective-permute-start = (bf16[16,256]{1,0:T(8,128)(2,1)S(1)}, bf16[16,256]{1,0:T(8,128)(2,1)S(1)}, u32[]{:S(2)}, u32[]{:S(2)}) collective-permute-start(bf16[16,256]{1,0:T(8,128)(2,1)S(1)} %get-tuple-element.35), channel_id=1, source_target_pairs={{0,16},{16,32},{32,48},{48,64},{64,80},{80,96},{96,112},{112,128},... | collective-permute-start | bytes 24584 | tf_op jit(solution)/shard_map/ppermute | solution.py:281
  15.5 6.8 %collective-permute-start.1 = (bf16[16,256]{1,0:T(8,128)(2,1)S(1)}, bf16[16,256]{1,0:T(8,128)(2,1)S(1)}, u32[]{:S(2)}, u32[]{:S(2)}) collective-permute-start(bf16[16,256]{1,0:T(8,128)(2,1)S(1)} %get-tuple-element.36), channel_id=1, source_target_pairs={{16,0},{32,16},{48,32},{64,48},{80,64},{96,80},{112,96},{128,112},... | collective-permute-start | bytes 24584 | tf_op jit(solution)/shard_map/ppermute | solution.py:282
  24.1 10.8 %collective-permute-start.2 = (bf16[736,256]{1,0:T(8,128)(2,1)}, bf16[736,256]{1,0:T(8,128)(2,1)}, u32[]{:S(2)}, u32[]{:S(2)}) collective-permute-start(bf16[736,256]{1,0:T(8,128)(2,1)} %pad_maximum_fusion), channel_id=1, source_target_pairs={{0,2},{1,3},{2,4},{3,5},{4,6},{5,7},{6,8},{7,9},{8,10},{9,11},{10,... | collective-permute-start | bytes 1130504 | tf_op jit(solution)/shard_map/ppermute | solution.py:32
  27.3 9.9 %collective-permute-start.3 = (bf16[736,256]{1,0:T(8,128)(2,1)}, bf16[736,256]{1,0:T(8,128)(2,1)}, u32[]{:S(2)}, u32[]{:S(2)}) collective-permute-start(bf16[736,256]{1,0:T(8,128)(2,1)} %pad_maximum_fusion), channel_id=1, source_target_pairs={{0,14},{1,15},{2,0},{3,1},{4,2},{5,3},{6,4},{7,5},{8,6},{9,7},{10,... | collective-permute-start | bytes 1130504 | tf_op jit(solution)/shard_map/ppermute | solution.py:32
  31.9 72.5 %copy-start.3 = (bf16[2,16,64,64]{3,2,1,0:T(8,128)(2,1)S(1)}, bf16[2,16,64,64]{3,2,1,0:T(8,128)(2,1)}, u32[]{:S(2)}) copy-start(bf16[2,16,64,64]{3,2,1,0:T(8,128)(2,1)} %param.10) | copy-start | bytes 786436
  34.8 10.7 %collective-permute-start.4 = (bf16[736,256]{1,0:T(8,128)(2,1)}, bf16[736,256]{1,0:T(8,128)(2,1)S(1)}, u32[]{:S(2)}, u32[]{:S(2)}) collective-permute-start(bf16[736,256]{1,0:T(8,128)(2,1)} %collective-permute-done.2), channel_id=1, source_target_pairs={{0,2},{1,3},{2,4},{3,5},{4,6},{5,7},{6,8},{7,9},{8,10},{9,11},{10,... | collective-permute-start | bytes 1130504 | tf_op jit(solution)/shard_map/ppermute | solution.py:32
  37.3 10.2 %collective-permute-start.5 = (bf16[736,256]{1,0:T(8,128)(2,1)}, bf16[736,256]{1,0:T(8,128)(2,1)S(1)}, u32[]{:S(2)}, u32[]{:S(2)}) collective-permute-start(bf16[736,256]{1,0:T(8,128)(2,1)} %collective-permute-done.3), channel_id=1, source_target_pairs={{0,14},{1,15},{2,0},{3,1},{4,2},{5,3},{6,4},{7,5},{8,6},{9,7},{10,... | collective-permute-start | bytes 1130504 | tf_op jit(solution)/shard_map/ppermute | solution.py:32
  45.5 9.6 %collective-permute-start.6 = (bf16[736,256]{1,0:T(8,128)(2,1)S(1)}, bf16[736,256]{1,0:T(8,128)(2,1)S(1)}, u32[]{:S(2)}, u32[]{:S(2)}) collective-permute-start(bf16[736,256]{1,0:T(8,128)(2,1)S(1)} %collective-permute-done.4), channel_id=1, source_target_pairs={{0,2},{1,3},{2,4},{3,5},{4,6},{5,7},{6,8},{7,9},{8,10},{9,11},{10,... | collective-permute-start | bytes 1130504 | tf_op jit(solution)/shard_map/ppermute | solution.py:32
  47.5 9.6 %collective-permute-start.7 = (bf16[736,256]{1,0:T(8,128)(2,1)S(1)}, bf16[736,256]{1,0:T(8,128)(2,1)S(1)}, u32[]{:S(2)}, u32[]{:S(2)}) collective-permute-start(bf16[736,256]{1,0:T(8,128)(2,1)S(1)} %collective-permute-done.5), channel_id=1, source_target_pairs={{0,14},{1,15},{2,0},{3,1},{4,2},{5,3},{6,4},{7,5},{8,6},{9,7},{10,... | collective-permute-start | bytes 1130504 | tf_op jit(solution)/shard_map/ppermute | solution.py:32
  55.1 9.6 %collective-permute-start.8 = (bf16[736,256]{1,0:T(8,128)(2,1)S(1)}, bf16[736,256]{1,0:T(8,128)(2,1)S(1)}, u32[]{:S(2)}, u32[]{:S(2)}) collective-permute-start(bf16[736,256]{1,0:T(8,128)(2,1)S(1)} %collective-permute-done.6), channel_id=1, source_target_pairs={{0,2},{1,3},{2,4},{3,5},{4,6},{5,7},{6,8},{7,9},{8,10},{9,11},{10,... | collective-permute-start | bytes 1130504 | tf_op jit(solution)/shard_map/ppermute | solution.py:32
  64.7 47.8 %copy-start = (bf16[8,736,256]{2,1,0:T(8,128)(2,1)}, bf16[8,736,256]{2,1,0:T(8,128)(2,1)S(1)}, u32[]{:S(2)}) copy-start(bf16[8,736,256]{2,1,0:T(8,128)(2,1)S(1)} %bitcast_dynamic-update-slice_fusion.refs_0_.refs_1_) | copy-start | bytes 9043972
  64.7 44.9 %collective-permute-start.9 = (bf16[8,736,256]{2,1,0:T(8,128)(2,1)S(1)}, bf16[8,736,256]{2,1,0:T(8,128)(2,1)}, u32[]{:S(2)}, u32[]{:S(2)}) collective-permute-start(bf16[8,736,256]{2,1,0:T(8,128)(2,1)S(1)} %bitcast_dynamic-update-slice_fusion.refs_0_.refs_1_), channel_id=1, source_target_pairs={{0,1},{1,0},{2,3},{3,2},{4,5},{5,4},{6,7},{7,6},{8,9},{9,8},{10,11... | collective-permute-start | bytes 9043976 | tf_op jit(solution)/shard_map/ppermute | solution.py:27
  119.2 40.9 %all-to-all-start = ((bf16[16,64,128]{2,1,0:T(8,128)(2,1)}), bf16[16,64,128]{2,1,0:T(8,128)(2,1)S(1)}, u32[]{:S(2)}, u32[]{:S(2)}) async-start(bf16[16,64,128]{2,1,0:T(8,128)(2,1)} %get-tuple-element.16), calls=%async_computation | async-start | bytes 524288 | tf_op jit(solution)/shard_map/all_to_all | solution.py:22
  162.5 4.5 %collective-permute-start.10 = (bf16[512,656]{0,1:T(8,128)(2,1)}, bf16[512,656]{0,1:T(8,128)(2,1)S(1)}, u32[]{:S(2)}, u32[]{:S(2)}) collective-permute-start(bf16[512,656]{0,1:T(8,128)(2,1)} %copy.15), channel_id=1, source_target_pairs={{0,1},{1,0},{2,3},{3,2},{4,5},{5,4},{6,7},{7,6},{8,9},{9,8},{10,11... | collective-permute-start | bytes 2015240 | tf_op jit(solution)/shard_map/ppermute | solution.py:27
  165.1 1.9 copy-start.2
  168.1 13.5 %all-to-all-start.1 = ((f32[16,1,656]{2,1,0:T(1,128)}), f32[16,1,656]{2,1,0:T(1,128)S(1)}, u32[]{:S(2)}, u32[]{:S(2)}) async-start(f32[16,1,656]{2,1,0:T(1,128)} %broadcast_in_dim.41), calls=%async_computation.1 | async-start | bytes 98304 | tf_op jit(solution)/shard_map/all_to_all | solution.py:18
  207.1 4.0 %collective-permute-start.11 = (bf16[512,640]{1,0:T(8,128)(2,1)S(1)}, bf16[512,640]{1,0:T(8,128)(2,1)S(1)}, u32[]{:S(2)}, u32[]{:S(2)}) collective-permute-start(bf16[512,640]{1,0:T(8,128)(2,1)S(1)} %all_gather.15), channel_id=1, source_target_pairs={{0,1},{1,0},{2,3},{3,2},{4,5},{5,4},{6,7},{7,6},{8,9},{9,8},{10,11... | collective-permute-start | bytes 1966088 | tf_op jit(solution)/shard_map/ppermute | solution.py:27
Sparse Core Ops, SparseCore 0:
  9.4 103.3 all-gather.2
